TPU v7x, 256 devices: a 4x2x16 block of a 4x16x16 slice. The times are simulated.
256 devices in a mesh: grp: 2 (over y), fs: 16 (over z), tp: 8 (over x, core).
Axes of the slice: x: 4, y: 2, z: 16, core: 2. Of those that a mesh axis runs over, the one named last changes fastest.
The devices are a block of a 4x16x16 slice.
Arguments:
- tokens: bfloat16 [32768, 2048], P(('grp', 'fs'), 'tp'), parts along dimension 0, may hold values from -50 to 50
- mix_gain: float32 [2048], replicated, may hold values from 0.1 to 1.9
- value_proj: bfloat16 [2048, 1024], P('fs', 'tp'), may hold values from -0.125 to 0.125
- gate_proj: bfloat16 [2048, 1024], P('fs', 'tp'), may hold values from -0.125 to 0.125
- conv_taps: float32 [31, 1024], P(None, 'tp'), may hold values from -1 to 1
- chan_gain: float32 [1024], replicated, may hold values from 0.1 to 1.9
- chan_shift: float32 [1024], replicated, may hold values from -3 to 3
- mix_out: bfloat16 [1024, 2048], P('fs', 'tp'), may hold values from -0.1875 to 0.1875
- mlp_gain: float32 [2048], replicated, may hold values from 0.1 to 1.9
- mlp_gate: bfloat16 [2048, 5632], P('fs', 'tp'), may hold values from -0.125 to 0.125
- mlp_up: bfloat16 [2048, 5632], P('fs', 'tp'), may hold values from -0.125 to 0.125
- gate_taps: float32 [3, 5632], P(None, 'tp'), may hold values from -3.5 to 3.5
- up_taps: float32 [3, 5632], P(None, 'tp'), may hold values from -3.5 to 3.5
- mlp_down: bfloat16 [5632, 2048], P('tp', 'fs'), may hold values from -0.078125 to 0.078125
- final_gain: float32 [2048], P('tp'), may hold values from 0.1 to 1.9
Outputs:
- layer_out: bfloat16 [32768, 2048], P(('grp', 'fs'), 'tp'), parts along dimension 0
There are 2 independent parts, one for each index of `grp`. A program takes and returns all parts, laid end to end along the dimension named above; an argument that names none is the same for every part. Nothing has to cross between parts.
All inputs are finite; a program needn't handle non-finite values.
Results may differ from a plain program's by a relative error of at most 0.0095.
Values may be sent and summed in bfloat16 or wider, within the bound.
A program may use at most 128 MiB of HBM per device.

v0:
```python
import jax
import jax.numpy as jnp
from jax import lax
from jax.sharding import PartitionSpec as P


def side_by_side(arrays, axis, dim, along):
    ends, at = ([], 0)
    for a in arrays[:-1]:
        at += a.shape[along]
        ends.append(at)
    both = jnp.concatenate(arrays, axis=along)
    return tuple(jnp.split(lax.all_gather(both, axis, axis=dim, tiled=True), ends, axis=along))


def rms_scale(values, gain):
    return values * lax.rsqrt(jnp.mean(values * values, axis=-1, keepdims=True) + 1e-06) * gain


def along_sequence(values, taps):
    width = taps.shape[0]
    half = (width - 1) // 2
    length = values.shape[0]
    padded = jnp.pad(values, ((half, width - 1 - half), (0, 0)))
    total = jnp.zeros_like(values)
    for offset in range(width):
        total = total + taps[offset] * padded[offset : offset + length]
    return total


def local(
    tokens,
    mix_gain,
    value_proj,
    gate_proj,
    conv_taps,
    chan_gain,
    chan_shift,
    mix_out,
    mlp_gain,
    mlp_gate,
    mlp_up,
    gate_taps,
    up_taps,
    mlp_down,
    final_gain,
):
    width_tp = lax.axis_size("tp")
    whole = lax.all_gather(tokens, "tp", axis=1, tiled=True)
    normed = rms_scale(whole.astype(jnp.float32), mix_gain).astype(jnp.bfloat16)
    first = jnp.dot(
        normed,
        lax.all_gather(value_proj, "fs", axis=0, tiled=True),
        preferred_element_type=jnp.float32,
    )
    second = jnp.dot(
        normed,
        lax.all_gather(gate_proj, "fs", axis=0, tiled=True),
        preferred_element_type=jnp.float32,
    )
    glu = first * jax.nn.sigmoid(second)
    conv_out = along_sequence(glu, conv_taps).astype(jnp.bfloat16)
    conv_all = lax.all_gather(conv_out, "tp", axis=1, tiled=True).astype(jnp.float32)
    mean = jnp.mean(conv_all, axis=-1, keepdims=True)
    var = jnp.mean(conv_all * conv_all, axis=-1, keepdims=True) - mean * mean
    chan_norm = (conv_all - mean) * lax.rsqrt(var + 1e-05) * chan_gain + chan_shift
    hidden_mix = jax.nn.silu(chan_norm).astype(jnp.bfloat16)
    mixer_result = jnp.dot(
        hidden_mix,
        lax.all_gather(mix_out, "fs", axis=0, tiled=True),
        preferred_element_type=jnp.float32,
    )
    mixed = (tokens.astype(jnp.float32) + mixer_result).astype(jnp.bfloat16)
    whole_two = lax.all_gather(mixed, "tp", axis=1, tiled=True)
    normed_two = rms_scale(whole_two.astype(jnp.float32), mlp_gain).astype(jnp.bfloat16)
    full_gate, full_up = side_by_side((mlp_gate, mlp_up), "fs", 0, 1)
    gate_pre = jnp.dot(normed_two, full_gate, preferred_element_type=jnp.float32)
    up_pre = jnp.dot(normed_two, full_up, preferred_element_type=jnp.float32)
    gate_conv = along_sequence(gate_pre, gate_taps)
    up_conv = along_sequence(up_pre, up_taps)
    hidden_mlp = (jax.nn.silu(gate_conv) * up_conv).astype(jnp.bfloat16)
    partial_terms = jnp.dot(
        hidden_mlp,
        lax.all_gather(mlp_down, "fs", axis=1, tiled=True),
        preferred_element_type=jnp.float32,
    )
    mlp_out = lax.psum_scatter(
        partial_terms.astype(jnp.bfloat16), "tp", scatter_dimension=1, tiled=True
    ).astype(jnp.float32)
    summed = mixed.astype(jnp.float32) + mlp_out
    squares = lax.psum(jnp.sum(summed * summed, axis=-1, keepdims=True), "tp")
    all_features = summed.shape[1] * width_tp
    layer_out = summed * lax.rsqrt(squares / all_features + 1e-06) * final_gain
    return layer_out.astype(jnp.bfloat16)


def solution(mesh):
    return jax.shard_map(
        local,
        mesh=mesh,
        in_specs=(
            P(("grp", "fs"), "tp"),
            P(),
            P("fs", "tp"),
            P("fs", "tp"),
            P(None, "tp"),
            P(),
            P(),
            P("fs", "tp"),
            P(),
            P("fs", "tp"),
            P("fs", "tp"),
            P(None, "tp"),
            P(None, "tp"),
            P("tp", "fs"),
            P("tp"),
        ),
        out_specs=P(("grp", "fs"), "tp"),
        check_vma=False,
    )
```

profile of v0, /device:TPU:33, one launch (start us, length us, event | category | flops | bytes accessed | tf_op | source)
XLA Modules:
  0.0 436.4 jit_solution(2931170777919696324)
XLA Ops:
  6.5 0.0 copy-start.11
  6.5 0.0 all-gather.6.cloned.1.call-start
  6.6 0.7 all-gather.6.cloned.1.call-update
  7.3 0.1 all-gather.8.cloned.1.call-start
  7.4 1.0 slice_bitcast_fusion.29
  8.3 1.0 slice_bitcast_fusion.30
  9.4 46.4 %all_gather.26 = bf16[2048,128]{1,0:T(8,128)(2,1)S(1)} all-gather(bf16[128,128]{1,0:T(8,128)(2,1)} %param.18), channel_id=1, replica_groups=mesh['grp'=2,'fs'=16,'tp'=8] {'fs'}, dimensions={0}, use_global_device_ids=true | all-gather | bytes 557056 | tf_op jit(solution)/shard_map/all_gather | solution.py:58
  55.7 23.2 %all_gather.25 = bf16[2048,128]{1,0:T(8,128)(2,1)S(1)} all-gather(bf16[128,128]{1,0:T(8,128)(2,1)} %param.17), channel_id=1, replica_groups=mesh['grp'=2,'fs'=16,'tp'=8] {'fs'}, dimensions={0}, use_global_device_ids=true | all-gather | bytes 557056 | tf_op jit(solution)/shard_map/all_gather | solution.py:53
  79.0 0.0 copy-start.1
  79.0 3.2 fusion
  82.2 0.0 copy-done.11
  82.2 0.2 copy-done.1
  82.4 1.3 fusion.41
  83.8 0.0 copy-start.3
  83.8 0.0 copy-start.6
  83.8 1.3 convolution_multiply_fusion
  85.1 0.0 copy-start.13
  85.1 0.0 copy-start.14
  85.1 2.8 add_convert_fusion
  87.9 0.1 all-gather.8.cloned.1.call-update
  88.0 0.1 all-gather.10.cloned.1.call-start
  88.1 0.0 copy-done.3
  88.1 0.2 copy.19
  88.3 0.0 copy-done.6
  88.3 23.6 %all_gather.28 = bf16[1024,256]{1,0:T(8,128)(2,1)S(1)} all-gather(bf16[64,256]{1,0:T(8,128)(2,1)S(1)} %copy-done.6), channel_id=1, replica_groups=mesh['grp'=2,'fs'=16,'tp'=8] {'fs'}, dimensions={0}, use_global_device_ids=true | all-gather | bytes 557056 | tf_op jit(solution)/shard_map/all_gather | solution.py:70
  111.9 16.1 %all-gather.8.cloned.1.call-done = bf16[1024,1024]{1,0:T(8,128)(2,1)} async-done(((bf16[1024,128]{1,0:T(8,128)(2,1)}), bf16[1024,1024]{1,0:T(8,128)(2,1)}) %all-gather.8.cloned.1.call-update) | async-done | bytes 2097168 | tf_op jit(solution)/shard_map/all_gather | solution.py:63
  128.1 2.3 convert_reduce_fusion
  130.4 0.0 copy-done.13
  130.4 0.0 copy-done.14
  130.4 0.0 copy-start.4
  130.4 0.0 copy-start.5
  130.4 0.0 copy-start.7
  130.4 0.0 copy-start.8
  130.4 4.4 %fusion.36 = bf16[1024,256]{0,1:T(8,128)(2,1)} fusion(bf16[1024,256]{1,0:T(8,128)(2,1)S(1)} %all_gather.28, bf16[1024,1024]{1,0:T(8,128)(2,1)} %all-gather.8.cloned.1.call-done, f32[1024]{0:T(1024)S(1)} %copy-done.13, f32[1024]{0:T(1024)S(1)} %copy-done.14, f32[1024]{0:T(1024)S(1)} %get-tuple-element.45, f32[1024]{0:T(1024)S(1)} %get-tuple-element.44, ...), kind=kOutput, calls=%fused_computation.44 | convolution fusion | flops 548143104 | bytes 3686400 | tf_op jit(solution)/shard_map/dot_general | solution.py:68
  134.8 0.1 all-gather.10.cloned.1.call-update
  134.9 0.1 all-gather.12.cloned.1.call-start
  135.0 0.0 copy-done.4
  135.0 0.0 copy-done.5
  135.0 0.8 pad_maximum_fusion
  135.8 0.1 all-gather.12.cloned.1.call-update
  135.8 0.1 all-gather.14.cloned.1.call-start
  135.9 0.6 all-gather.14.cloned.1.call-update
  136.5 0.2 reduce-scatter.2.cloned.1.call-start
  136.7 0.0 copy-done.7
  136.7 0.0 copy-done.8
  136.8 0.1 slice_reduce_fusion.2
  136.8 36.9 %all-gather.10.cloned.1.call-done = bf16[1024,2048]{0,1:T(8,128)(2,1)} async-done(((bf16[1024,256]{0,1:T(8,128)(2,1)}), bf16[1024,2048]{0,1:T(8,128)(2,1)}) %all-gather.10.cloned.1.call-update) | async-done | bytes 4194320 | tf_op jit(solution)/shard_map/all_gather | solution.py:74
  173.7 3.1 fusion.3
  176.8 93.9 %all-gather.12.cloned.1.call-done = bf16[2048,1408]{0,1:T(8,128)(2,1)} async-done(((bf16[128,1408]{0,1:T(8,128)(2,1)}), bf16[2048,1408]{0,1:T(8,128)(2,1)}) %all-gather.12.cloned.1.call-update) | async-done | bytes 5767184 | tf_op jit(solution)/shard_map/all_gather | solution.py:13
  270.7 0.0 copy-done.12
  270.7 6.4 %fusion.28 = f32[1024,704]{0,1:T(8,128)S(1)} fusion(bf16[2048,1408]{0,1:T(8,128)(2,1)} %all-gather.12.cloned.1.call-done, bf16[1024,2048]{0,1:T(8,128)(2,1)} %all-gather.10.cloned.1.call-done, f32[2048]{0:T(1024)S(1)} %copy-done.12, f32[1024]{0:T(1024)S(1)} %add_rsqrt_fusion.1), kind=kOutput, calls=%fused_computation.40 | convolution fusion | flops 2961178624 | bytes 9973760 | tf_op jit(solution)/shard_map/dot_general | solution.py:77
  277.1 0.0 copy-done.2
  277.1 0.0 copy-done.10
  277.1 4.8 %fusion.26 = f32[1024,704]{0,1:T(8,128)} fusion(bf16[2048,1408]{0,1:T(8,128)(2,1)S(1)} %copy-done.10, bf16[1024,2048]{0,1:T(8,128)(2,1)S(1)} %copy-done.2, f32[2048]{0:T(1024)S(1)} %copy-done.12, f32[1024]{0:T(1024)S(1)} %add_rsqrt_fusion.1), kind=kOutput, calls=%fused_computation.38 | convolution fusion | flops 2961178624 | bytes 9973760 | tf_op jit(solution)/shard_map/dot_general | solution.py:78
  282.0 68.3 %all-gather.14.cloned.1.call-done = bf16[704,2048]{1,0:T(8,128)(2,1)} async-done(((bf16[704,128]{1,0:T(8,128)(2,1)}), bf16[704,2048]{1,0:T(8,128)(2,1)}) %all-gather.14.cloned.1.call-update) | async-done | bytes 2883600 | tf_op jit(solution)/shard_map/all_gather | solution.py:84
  350.3 12.2 %convolution_convert_fusion = bf16[1024,2048]{0,1:T(8,128)(2,1)} fusion(bf16[704,2048]{1,0:T(8,128)(2,1)} %all-gather.14.cloned.1.call-done, f32[1024,704]{0,1:T(8,128)} %fusion.26, f32[1024,704]{0,1:T(8,128)S(1)} %fusion.28, f32[704]{0:T(1024)S(1)} %get-tuple-element.11, f32[704]{0:T(1024)S(1)} %get-tuple-element.12, f32[704]{0:T(1024)S(1)} %get-tuple-element.10, ...), kind=kOutput, calls=%fused_computation.23 | convolution fusion | flops 2966421504 | bytes 12861952 | tf_op jit(solution)/shard_map/dot_general | solution.py:82
  362.4 0.1 reduce-scatter.2.cloned.1.call-update
  362.5 48.7 %reduce-scatter.2.cloned.1.call-done = bf16[1024,256]{0,1:T(8,128)(2,1)} async-done(((bf16[1024,2048]{0,1:T(8,128)(2,1)}), bf16[1024,256]{0,1:T(8,128)(2,1)}) %reduce-scatter.2.cloned.1.call-update) | async-done | bytes 524304 | tf_op jit(solution)/shard_map/reduce_scatter | solution.py:87
  411.2 0.0 copy-done
  411.2 1.2 multiply_reduce_fusion
  412.4 14.8 %psum.7 = f32[1024,1]{0,1:T(1,128)S(1)} all-reduce(f32[1024,1]{0,1:T(1,128)S(1)} %bitcast.69), channel_id=1, replica_groups=mesh['grp'=2,'fs'=16,'tp'=8] {'tp'}, use_global_device_ids=true, to_apply=%region_6.7 | all-reduce | flops 1024 | bytes 8192 | tf_op jit(solution)/shard_map/psum | solution.py:91
  427.3 0.0 copy-done.9
  427.3 1.2 multiply_convert_fusion
  428.5 1.0 copy.21
  (10 shorter events, 0.0 us)
Async XLA Ops:
  6.5 75.7 %copy-start.11 = (f32[2048]{0:T(1024)S(1)}, f32[2048]{0:T(1024)}, u32[]{:S(2)}) copy-start(f32[2048]{0:T(1024)} %param.16) | copy-start | bytes 24580
  6.5 72.4 %all-gather.6.cloned.1.call-start = ((), (), s32[]{:S(2)}) async-start(), calls=%async_computation.1 | async-start | bytes 4718592 | tf_op jit(solution)/shard_map/all_gather | solution.py:49
  7.3 120.8 %all-gather.8.cloned.1.call-start = ((), (), s32[]{:S(2)}) async-start(), calls=%async_computation.2 | async-start | bytes 2359296 | tf_op jit(solution)/shard_map/all_gather | solution.py:63
  79.0 3.5 copy-start.1
  83.8 4.3 copy-start.3
  83.8 4.5 %copy-start.6 = (bf16[64,256]{1,0:T(8,128)(2,1)S(1)}, bf16[64,256]{1,0:T(8,128)(2,1)}, u32[]{:S(2)}) copy-start(bf16[64,256]{1,0:T(8,128)(2,1)} %param.22) | copy-start | bytes 98308
  85.1 45.2 %copy-start.13 = (f32[1024]{0:T(1024)S(1)}, f32[1024]{0:T(1024)}, u32[]{:S(2)}) copy-start(f32[1024]{0:T(1024)} %param.21) | copy-start | bytes 12292
  85.1 45.2 %copy-start.14 = (f32[1024]{0:T(1024)S(1)}, f32[1024]{0:T(1024)}, u32[]{:S(2)}) copy-start(f32[1024]{0:T(1024)} %param.20) | copy-start | bytes 12292
  88.0 85.7 %all-gather.10.cloned.1.call-start = ((), (), s32[]{:S(2)}) async-start(), calls=%async_computation.3 | async-start | bytes 4718592 | tf_op jit(solution)/shard_map/all_gather | solution.py:74
  130.4 4.6 %copy-start.4 = (bf16[128,704]{0,1:T(8,128)(2,1)S(1)}, bf16[128,704]{0,1:T(8,128)(2,1)}, u32[]{:S(2)}) copy-start(bf16[128,704]{0,1:T(8,128)(2,1)} %param.25) | copy-start | bytes 540676
  130.4 4.6 %copy-start.5 = (bf16[128,704]{0,1:T(8,128)(2,1)S(1)}, bf16[128,704]{0,1:T(8,128)(2,1)}, u32[]{:S(2)}) copy-start(bf16[128,704]{0,1:T(8,128)(2,1)} %param.24) | copy-start | bytes 540676
  130.4 6.3 %copy-start.7 = (f32[3,704]{1,0:T(4,128)S(1)}, f32[3,704]{1,0:T(4,128)}, u32[]{:S(2)}) copy-start(f32[3,704]{1,0:T(4,128)} %param.27) | copy-start | bytes 25348
  130.4 6.3 %copy-start.8 = (f32[3,704]{1,0:T(4,128)S(1)}, f32[3,704]{1,0:T(4,128)}, u32[]{:S(2)}) copy-start(f32[3,704]{1,0:T(4,128)} %param.26) | copy-start | bytes 25348
  134.8 135.8 %copy-start.12 = (f32[2048]{0:T(1024)S(1)}, f32[2048]{0:T(1024)}, u32[]{:S(2)}) copy-start(f32[2048]{0:T(1024)} %param.23) | copy-start | bytes 24580
  134.9 135.8 %all-gather.12.cloned.1.call-start = ((), (), s32[]{:S(2)}) async-start(), calls=%async_computation.4 | async-start | bytes 6127616 | tf_op jit(solution)/shard_map/all_gather | solution.py:13
  135.8 214.4 %all-gather.14.cloned.1.call-start = ((), (), s32[]{:S(2)}) async-start(), calls=%async_computation.5 | async-start | bytes 3063808 | tf_op jit(solution)/shard_map/all_gather | solution.py:84
  136.5 274.7 %reduce-scatter.2.cloned.1.call-start = ((), (), s32[]{:S(2)}) async-start(), calls=%async_computation.6 | async-start | bytes 4718592 | tf_op jit(solution)/shard_map/reduce_scatter | solution.py:87
  270.7 6.4 %copy-start.2 = (bf16[1024,2048]{0,1:T(8,128)(2,1)S(1)}, bf16[1024,2048]{0,1:T(8,128)(2,1)}, u32[]{:S(2)}) copy-start(bf16[1024,2048]{0,1:T(8,128)(2,1)} %all-gather.10.cloned.1.call-done) | copy-start | bytes 12582916
  270.7 6.5 %copy-start.10 = (bf16[2048,1408]{0,1:T(8,128)(2,1)S(1)}, bf16[2048,1408]{0,1:T(8,128)(2,1)}, u32[]{:S(2)}) copy-start(bf16[2048,1408]{0,1:T(8,128)(2,1)} %all-gather.12.cloned.1.call-done) | copy-start | bytes 17301508
  362.4 48.8 %copy-start = (bf16[1024,256]{0,1:T(8,128)(2,1)S(1)}, bf16[1024,256]{0,1:T(8,128)(2,1)}, u32[]{:S(2)}) copy-start(bf16[1024,256]{0,1:T(8,128)(2,1)} %fusion.36) | copy-start | bytes 1572868
  362.4 64.8 %copy-start.9 = (f32[256]{0:T(256)S(1)}, f32[256]{0:T(256)}, u32[]{:S(2)}) copy-start(f32[256]{0:T(256)} %param.29) | copy-start | bytes 3076
Sparse Core Ops, SparseCore 0:
  9.2 56.5 all-gather.5
  88.1 39.9 all-gather.7
  135.0 38.6 all-gather.9
  175.3 95.3 all-gather.11
  272.3 77.9 all-gather.13
  362.6 48.5 reduce-scatter.1
where the time goes:
time: 437 us; the launch traced here: 436 us
  waiting for transfers between devices  265 us (61%)
  blocking collectives  108 us (25%)
  matrix products  30.5 us (7%)
  other arithmetic  14.7 us (3%)
  between operations  13.7 us (3%)
    all_gather x1, waiting for transfers between devices, side_by_side(): lax.all_gather(both, axis, axis=dim, tiled=True)  93.9 us
    all_gather x1, waiting for transfers between devices, local(): lax.all_gather(mlp_down, 'fs', axis=1, tiled=True)  68.3 us
    reduce_scatter x1, waiting for transfers between devices, local(): lax.psum_scatter(partial_terms.astype(jnp.bfloat16), 'tp', scatter_dimens...  48.7 us
    all_gather x1, blocking collectives, local(): lax.all_gather(gate_proj, 'fs', axis=0, tiled=True)  46.4 us
    all_gather x1, waiting for transfers between devices, local(): whole_two = lax.all_gather(mixed, 'tp', axis=1, tiled=True)  36.9 us
    all_gather x1, blocking collectives, local(): lax.all_gather(mix_out, 'fs', axis=0, tiled=True)  23.6 us
    all_gather x1, blocking collectives, local(): lax.all_gather(value_proj, 'fs', axis=0, tiled=True)  23.2 us
    all_gather x1, waiting for transfers between devices, local(): lax.all_gather(conv_out, 'tp', axis=1, tiled=True).astype(jnp.float32)  16.1 us
  transfers between devices with their start and end apart: 6, of which 5 were waited for; matrix products, arithmetic and copies ran while one was open for 4% of the time, Pallas kernels for 0%

commit v1 on v0

--- a/solution.py
+++ b/solution.py
@@ -79,10 +79,11 @@
     gate_conv = along_sequence(gate_pre, gate_taps)
     up_conv = along_sequence(up_pre, up_taps)
     hidden_mlp = (jax.nn.silu(gate_conv) * up_conv).astype(jnp.bfloat16)
+    expand_series_all = lambda x_local, which_dim: jnp.concatenate(
+        lax.all_to_all(jnp.stack(lax.axis_size("fs") * [x_local]), "fs", 0, 0), axis=which_dim
+    )
     partial_terms = jnp.dot(
-        hidden_mlp,
-        lax.all_gather(mlp_down, "fs", axis=1, tiled=True),
-        preferred_element_type=jnp.float32,
+        hidden_mlp, expand_series_all(mlp_down, 1), preferred_element_type=jnp.float32
     )
     mlp_out = lax.psum_scatter(
         partial_terms.astype(jnp.bfloat16), "tp", scatter_dimension=1, tiled=True

time: 437 us -> 447 us (1.023)
  starting transfers between devices: 0.5 us -> 12.2 us
  waiting for transfers between devices: 265 us -> 259 us
    all_gather x1, waiting for transfers between devices: 93.9 us -> 174 us  [side_by_side(): lax.all_gather(both, axis, axis=dim, tiled=True)]
    all_gather x1 -> x0, waiting for transfers between devices: 68.3 us -> none  [local(): lax.all_gather(mlp_down, 'fs', axis=1, tiled=True)]
    all_gather x1, waiting for transfers between devices: 36.9 us -> 23.6 us  [local(): whole_two = lax.all_gather(mixed, 'tp', axis=1, tiled=True)]
    all_to_all x0 -> x1, starting transfers between devices: none -> 11.8 us  [local(): lax.all_to_all(jnp.stack(lax.axis_size('fs') * [x_local]), 'fs', 0, 0)]
  transfers between devices with their start and end apart: 6 -> 6, of which waited for: 5 -> 4; matrix products, arithmetic and copies ran while one was open for 4% -> 5% of each run, Pallas kernels for 0% -> 0%
where the time goes in v1:
time: 447 us
  waiting for transfers between devices  259 us (58%)
  blocking collectives  108 us (24%)
  matrix products  33.4 us (7%)
  other arithmetic  14.7 us (3%)
  between operations  13.4 us (3%)
  starting transfers between devices  12.2 us (3%)
  local copies, waits for them, and re-layouts  5.64 us (1%)
    all_gather x1, waiting for transfers between devices, side_by_side(): lax.all_gather(both, axis, axis=dim, tiled=True)  174 us
    all_gather x1, blocking collectives, local(): lax.all_gather(gate_proj, 'fs', axis=0, tiled=True)  46.4 us
    reduce_scatter x1, waiting for transfers between devices, local(): lax.psum_scatter(partial_terms.astype(jnp.bfloat16), 'tp', scatter_dimens...  44.4 us
    all_gather x1, blocking collectives, local(): lax.all_gather(mix_out, 'fs', axis=0, tiled=True)  23.6 us
    all_gather x1, waiting for transfers between devices, local(): whole_two = lax.all_gather(mixed, 'tp', axis=1, tiled=True)  23.6 us
    all_gather x1, blocking collectives, local(): lax.all_gather(value_proj, 'fs', axis=0, tiled=True)  23.2 us
    all_gather x1, waiting for transfers between devices, local(): lax.all_gather(conv_out, 'tp', axis=1, tiled=True).astype(jnp.float32)  16.1 us
    psum x1, blocking collectives, local(): squares = lax.psum(jnp.sum(summed * summed, axis=-1, keepdims=True), 'tp')  14.8 us
  transfers between devices with their start and end apart: 6, of which 4 were waited for; matrix products, arithmetic and copies ran while one was open for 5% of the time, Pallas kernels for 0%

profile of v1, /device:TPU:33, one launch (start us, length us, event | category | flops | bytes accessed | tf_op | source)
XLA Modules:
  0.0 446.7 jit_solution(15566416436545558179)
XLA Ops:
  6.5 0.0 all-gather.5.cloned.1.call-start
  6.6 0.7 all-gather.5.cloned.1.call-update
  7.3 0.1 all-gather.7.cloned.1.call-start
  7.4 1.0 slice_bitcast_fusion.29
  8.3 1.0 slice_bitcast_fusion.30
  9.4 46.4 %all_gather.23 = bf16[2048,128]{1,0:T(8,128)(2,1)S(1)} all-gather(bf16[128,128]{1,0:T(8,128)(2,1)} %param.18), channel_id=1, replica_groups=mesh['grp'=2,'fs'=16,'tp'=8] {'fs'}, dimensions={0}, use_global_device_ids=true | all-gather | bytes 557056 | tf_op jit(solution)/shard_map/all_gather | solution.py:58
  55.7 23.2 %all_gather.22 = bf16[2048,128]{1,0:T(8,128)(2,1)S(1)} all-gather(bf16[128,128]{1,0:T(8,128)(2,1)} %param.17), channel_id=1, replica_groups=mesh['grp'=2,'fs'=16,'tp'=8] {'fs'}, dimensions={0}, use_global_device_ids=true | all-gather | bytes 557056 | tf_op jit(solution)/shard_map/all_gather | solution.py:53
  79.0 3.2 fusion
  82.2 0.0 copy-done.12
  82.2 0.2 copy-done.1
  82.4 1.3 fusion.43
  83.8 0.0 copy-start.3
  83.8 0.0 copy-start.7
  83.8 1.3 convolution_multiply_fusion
  85.1 0.0 copy-start.14
  85.1 0.0 copy-start.15
  85.1 2.8 add_convert_fusion
  87.9 0.1 all-gather.7.cloned.1.call-update
  88.0 0.1 all-gather.9.cloned.1.call-start
  88.1 0.0 copy-done.3
  88.1 0.2 copy.22
  88.3 0.0 copy-done.7
  88.3 23.6 %all_gather.25 = bf16[1024,256]{1,0:T(8,128)(2,1)S(1)} all-gather(bf16[64,256]{1,0:T(8,128)(2,1)S(1)} %copy-done.7), channel_id=1, replica_groups=mesh['grp'=2,'fs'=16,'tp'=8] {'fs'}, dimensions={0}, use_global_device_ids=true | all-gather | bytes 557056 | tf_op jit(solution)/shard_map/all_gather | solution.py:70
  111.9 16.1 %all-gather.7.cloned.1.call-done = bf16[1024,1024]{1,0:T(8,128)(2,1)} async-done(((bf16[1024,128]{1,0:T(8,128)(2,1)}), bf16[1024,1024]{1,0:T(8,128)(2,1)}) %all-gather.7.cloned.1.call-update) | async-done | bytes 2097168 | tf_op jit(solution)/shard_map/all_gather | solution.py:63
  128.1 2.3 convert_reduce_fusion
  130.4 0.0 copy-done.14
  130.4 0.0 copy-done.15
  130.4 0.0 copy-start.4
  130.4 0.0 copy-start.5
  130.4 0.0 copy-start.6
  130.4 4.4 fusion.38
  134.8 0.1 all-gather.9.cloned.1.call-update
  134.9 0.1 all-gather.11.cloned.1.call-start
  134.9 0.0 copy-done.4
  134.9 0.0 copy-done.5
  134.9 0.8 pad_maximum_fusion
  135.7 0.1 all-gather.11.cloned.1.call-update
  135.8 0.0 copy-done.6
  135.8 0.0 copy-start.8
  135.8 0.0 copy-start.9
  135.8 2.1 stack.2
  137.9 11.8 %all-to-all-start = ((bf16[16,704,128]{2,1,0:T(8,128)(2,1)}), bf16[16,704,128]{2,1,0:T(8,128)(2,1)S(1)}, u32[]{:S(2)}, u32[]{:S(2)}) async-start(bf16[16,704,128]{2,1,0:T(8,128)(2,1)} %stack.2), calls=%async_computation | async-start | bytes 5767168 | tf_op jit(solution)/shard_map/all_to_all | solution.py:83
  149.7 0.2 reduce-scatter.2.cloned.1.call-start
  150.0 0.0 copy-done.8
  150.0 0.0 copy-done.9
  150.0 0.1 slice_reduce_fusion.2
  150.1 23.6 %all-gather.9.cloned.1.call-done = bf16[1024,2048]{0,1:T(8,128)(2,1)} async-done(((bf16[1024,256]{0,1:T(8,128)(2,1)}), bf16[1024,2048]{0,1:T(8,128)(2,1)}) %all-gather.9.cloned.1.call-update) | async-done | bytes 4194320 | tf_op jit(solution)/shard_map/all_gather | solution.py:74
  173.7 3.1 fusion.3
  176.8 174.1 %all-gather.11.cloned.1.call-done = bf16[2048,1408]{0,1:T(8,128)(2,1)} async-done(((bf16[128,1408]{0,1:T(8,128)(2,1)}), bf16[2048,1408]{0,1:T(8,128)(2,1)}) %all-gather.11.cloned.1.call-update) | async-done | bytes 5767184 | tf_op jit(solution)/shard_map/all_gather | solution.py:13
  350.9 0.0 copy-done.13
  350.9 8.0 %fusion.30 = f32[1024,704]{0,1:T(8,128)} fusion(bf16[2048,1408]{0,1:T(8,128)(2,1)} %all-gather.11.cloned.1.call-done, bf16[1024,2048]{0,1:T(8,128)(2,1)} %all-gather.9.cloned.1.call-done, f32[2048]{0:T(1024)S(1)} %copy-done.13, f32[1024]{0:T(1024)S(1)} %add_rsqrt_fusion.1), kind=kOutput, calls=%fused_computation.42 | convolution fusion | flops 2961178624 | bytes 9973760 | tf_op jit(solution)/shard_map/dot_general | solution.py:77
  358.9 0.0 copy-done.2
  358.9 0.0 copy-done.11
  358.9 4.8 %fusion.28 = f32[1024,704]{0,1:T(8,128)} fusion(bf16[2048,1408]{0,1:T(8,128)(2,1)S(1)} %copy-done.11, bf16[1024,2048]{0,1:T(8,128)(2,1)S(1)} %copy-done.2, f32[2048]{0:T(1024)S(1)} %copy-done.13, f32[1024]{0:T(1024)S(1)} %add_rsqrt_fusion.1), kind=kOutput, calls=%fused_computation.40 | convolution fusion | flops 2961178624 | bytes 9973760 | tf_op jit(solution)/shard_map/dot_general | solution.py:78
  363.7 0.0 all-to-all-done
  363.7 13.6 %convolution_convert_fusion = bf16[1024,2048]{0,1:T(8,128)(2,1)} fusion(f32[1024,704]{0,1:T(8,128)} %fusion.28, f32[1024,704]{0,1:T(8,128)} %fusion.30, f32[704]{0:T(1024)S(1)} %get-tuple-element.11, f32[704]{0:T(1024)S(1)} %get-tuple-element.12, f32[704]{0:T(1024)S(1)} %get-tuple-element.10, f32[704]{0:T(1024)S(1)} %get-tuple-element.47, ...), kind=kOutput, calls=%fused_computation.23 | convolution fusion | flops 2966421504 | bytes 12861952 | tf_op jit(solution)/shard_map/dot_general | solution.py:85
  377.3 0.1 reduce-scatter.2.cloned.1.call-update
  377.4 44.4 %reduce-scatter.2.cloned.1.call-done = bf16[1024,256]{0,1:T(8,128)(2,1)} async-done(((bf16[1024,2048]{0,1:T(8,128)(2,1)}), bf16[1024,256]{0,1:T(8,128)(2,1)}) %reduce-scatter.2.cloned.1.call-update) | async-done | bytes 524304 | tf_op jit(solution)/shard_map/reduce_scatter | solution.py:88
  421.8 0.0 copy-done
  421.8 1.2 multiply_reduce_fusion
  423.0 14.8 %psum.7 = f32[1024,1]{0,1:T(1,128)S(1)} all-reduce(f32[1024,1]{0,1:T(1,128)S(1)} %bitcast.76), channel_id=1, replica_groups=mesh['grp'=2,'fs'=16,'tp'=8] {'tp'}, use_global_device_ids=true, to_apply=%region_6.7 | all-reduce | flops 1024 | bytes 8192 | tf_op jit(solution)/shard_map/psum | solution.py:92
  437.9 0.0 copy-done.10
  437.9 1.2 multiply_convert_fusion
  439.1 1.0 copy.25
  (12 shorter events, 0.1 us)
Async XLA Ops:
  6.5 75.7 %copy-start.12 = (f32[2048]{0:T(1024)S(1)}, f32[2048]{0:T(1024)}, u32[]{:S(2)}) copy-start(f32[2048]{0:T(1024)} %param.16) | copy-start | bytes 24580
  6.5 72.4 %all-gather.5.cloned.1.call-start = ((), (), s32[]{:S(2)}) async-start(), calls=%async_computation.2 | async-start | bytes 4718592 | tf_op jit(solution)/shard_map/all_gather | solution.py:49
  7.3 120.8 %all-gather.7.cloned.1.call-start = ((), (), s32[]{:S(2)}) async-start(), calls=%async_computation.3 | async-start | bytes 2359296 | tf_op jit(solution)/shard_map/all_gather | solution.py:63
  79.0 3.5 copy-start.1
  83.8 4.3 copy-start.3
  83.8 4.5 %copy-start.7 = (bf16[64,256]{1,0:T(8,128)(2,1)S(1)}, bf16[64,256]{1,0:T(8,128)(2,1)}, u32[]{:S(2)}) copy-start(bf16[64,256]{1,0:T(8,128)(2,1)} %param.22) | copy-start | bytes 98308
  85.1 45.2 %copy-start.14 = (f32[1024]{0:T(1024)S(1)}, f32[1024]{0:T(1024)}, u32[]{:S(2)}) copy-start(f32[1024]{0:T(1024)} %param.21) | copy-start | bytes 12292
  85.1 45.2 %copy-start.15 = (f32[1024]{0:T(1024)S(1)}, f32[1024]{0:T(1024)}, u32[]{:S(2)}) copy-start(f32[1024]{0:T(1024)} %param.20) | copy-start | bytes 12292
  88.0 85.7 %all-gather.9.cloned.1.call-start = ((), (), s32[]{:S(2)}) async-start(), calls=%async_computation.4 | async-start | bytes 4718592 | tf_op jit(solution)/shard_map/all_gather | solution.py:74
  130.4 4.6 %copy-start.4 = (bf16[128,704]{0,1:T(8,128)(2,1)S(1)}, bf16[128,704]{0,1:T(8,128)(2,1)}, u32[]{:S(2)}) copy-start(bf16[128,704]{0,1:T(8,128)(2,1)} %param.25) | copy-start | bytes 540676
  130.4 4.6 %copy-start.5 = (bf16[128,704]{0,1:T(8,128)(2,1)S(1)}, bf16[128,704]{0,1:T(8,128)(2,1)}, u32[]{:S(2)}) copy-start(bf16[128,704]{0,1:T(8,128)(2,1)} %param.24) | copy-start | bytes 540676
  130.4 5.4 %copy-start.6 = (bf16[704,128]{1,0:T(8,128)(2,1)S(1)}, bf16[704,128]{1,0:T(8,128)(2,1)}, u32[]{:S(2)}) copy-start(bf16[704,128]{1,0:T(8,128)(2,1)} %param.28) | copy-start | bytes 540676
  134.9 216.0 %all-gather.11.cloned.1.call-start = ((), (), s32[]{:S(2)}) async-start(), calls=%async_computation.5 | async-start | bytes 6127616 | tf_op jit(solution)/shard_map/all_gather | solution.py:13
  135.8 14.2 %copy-start.8 = (f32[3,704]{1,0:T(4,128)S(1)}, f32[3,704]{1,0:T(4,128)}, u32[]{:S(2)}) copy-start(f32[3,704]{1,0:T(4,128)} %param.27) | copy-start | bytes 25348
  135.8 14.2 %copy-start.9 = (f32[3,704]{1,0:T(4,128)S(1)}, f32[3,704]{1,0:T(4,128)}, u32[]{:S(2)}) copy-start(f32[3,704]{1,0:T(4,128)} %param.26) | copy-start | bytes 25348
  137.9 213.0 %copy-start.13 = (f32[2048]{0:T(1024)S(1)}, f32[2048]{0:T(1024)}, u32[]{:S(2)}) copy-start(f32[2048]{0:T(1024)} %param.23) | copy-start | bytes 24580
  137.9 225.8 %all-to-all-start = ((bf16[16,704,128]{2,1,0:T(8,128)(2,1)}), bf16[16,704,128]{2,1,0:T(8,128)(2,1)S(1)}, u32[]{:S(2)}, u32[]{:S(2)}) async-start(bf16[16,704,128]{2,1,0:T(8,128)(2,1)} %stack.2), calls=%async_computation | async-start | bytes 5767168 | tf_op jit(solution)/shard_map/all_to_all | solution.py:83
  149.7 272.1 %reduce-scatter.2.cloned.1.call-start = ((), (), s32[]{:S(2)}) async-start(), calls=%async_computation.6 | async-start | bytes 4718592 | tf_op jit(solution)/shard_map/reduce_scatter | solution.py:88
  350.9 8.0 %copy-start.2 = (bf16[1024,2048]{0,1:T(8,128)(2,1)S(1)}, bf16[1024,2048]{0,1:T(8,128)(2,1)}, u32[]{:S(2)}) copy-start(bf16[1024,2048]{0,1:T(8,128)(2,1)} %all-gather.9.cloned.1.call-done) | copy-start | bytes 12582916
  350.9 8.0 %copy-start.11 = (bf16[2048,1408]{0,1:T(8,128)(2,1)S(1)}, bf16[2048,1408]{0,1:T(8,128)(2,1)}, u32[]{:S(2)}) copy-start(bf16[2048,1408]{0,1:T(8,128)(2,1)} %all-gather.11.cloned.1.call-done) | copy-start | bytes 17301508
  377.3 44.5 %copy-start = (bf16[1024,256]{0,1:T(8,128)(2,1)S(1)}, bf16[1024,256]{0,1:T(8,128)(2,1)}, u32[]{:S(2)}) copy-start(bf16[1024,256]{0,1:T(8,128)(2,1)} %fusion.38) | copy-start | bytes 1572868
  377.3 60.6 %copy-start.10 = (f32[256]{0:T(256)S(1)}, f32[256]{0:T(256)}, u32[]{:S(2)}) copy-start(f32[256]{0:T(256)} %param.29) | copy-start | bytes 3076
Sparse Core Ops, SparseCore 0:
  9.2 56.5 all-gather.4
  88.1 39.9 all-gather.6
  135.0 38.6 all-gather.8
  175.3 175.5 all-gather.10
  377.5 44.2 reduce-scatter.1
